TPU v7x, 32 devices: a whole 2x2x4 slice. The times are simulated.
32 devices in a mesh: sp: 16 (over z, y, core), tp: 2 (over x).
Axes of the slice: x: 2, y: 2, z: 4, core: 2. Of those that a mesh axis runs over, the one named last changes fastest.
Arguments:
- stream: bfloat16 [2048, 2048], P('sp', 'tp'), may hold values from -52 to 52
- norm_gain: float32 [2, 2048], replicated, may hold values from 0.1 to 1.9
- value_weight: bfloat16 [4096, 1024], P('sp', 'tp'), may hold values from -0.125 to 0.125
- gate_weight: bfloat16 [4096, 1024], P('sp', 'tp'), may hold values from -0.125 to 0.125
- conv_taps: float32 [2, 31, 1024], replicated, may hold values from -3 to 3
- ln_gain: float32 [2, 1024], replicated, may hold values from 0.1 to 1.9
- ln_bias: float32 [2, 1024], replicated, may hold values from -3 to 3
- out_weight: bfloat16 [1024, 4096], P('tp', 'sp'), may hold values from -0.1875 to 0.1875
- final_gain: float32 [2048], replicated, may hold values from 0.1 to 1.9
Outputs:
- result: bfloat16 [2048, 2048], P('sp', 'tp')
All inputs are finite; a program needn't handle non-finite values.
Results may differ from a plain program's by a relative error of at most 0.014.
Values may be sent and summed in bfloat16 or wider, within the bound.
A program may use at most 64 MiB of HBM per device.

v0:
```python
import jax
import jax.numpy as jnp
from jax import lax
from jax.sharding import PartitionSpec as P

D = 2048
C = 1024
KW = 31
LAYERS = 2


EPS = 1e-06


def from_behind(value, axis, steps):
    count = lax.axis_size(axis)
    first, last = (max(0, -steps), min(count, count - steps))
    return lax.ppermute(value, axis, [(source, source + steps) for source in range(first, last)])


def valid_conv(extended, tap_table):
    length = extended.shape[0] - (KW - 1)
    running = tap_table[0] * extended[0:length]
    for tap_index in range(1, KW):
        running = running + tap_table[tap_index] * extended[tap_index : tap_index + length]
    return running


def local(
    stream,
    norm_gain,
    value_weight,
    gate_weight,
    conv_taps,
    ln_gain,
    ln_bias,
    out_weight,
    final_gain,
):
    tokens_here = stream.shape[0]
    columns = stream.shape[1]
    channels = value_weight.shape[1]
    rim_rows = KW - 1
    tp_index = lax.axis_index("tp")
    my_taps = lax.dynamic_slice_in_dim(conv_taps, tp_index * channels, channels, 2)
    my_ln_gain = lax.dynamic_slice_in_dim(ln_gain, tp_index * channels, channels, 1)
    my_ln_bias = lax.dynamic_slice_in_dim(ln_bias, tp_index * channels, channels, 1)
    my_final = lax.dynamic_slice_in_dim(final_gain, tp_index * columns, columns, 0)
    value_all, gate_all, out_all = (
        lax.all_gather(value_weight, "sp", axis=0, tiled=True),
        lax.all_gather(gate_weight, "sp", axis=0, tiled=True),
        lax.all_gather(out_weight, "sp", axis=1, tiled=True),
    )
    value_all = value_all.reshape(D, LAYERS, channels)
    gate_all = gate_all.reshape(D, LAYERS, channels)
    out_all = out_all.reshape(channels, D, LAYERS)
    earlier = from_behind(stream[-LAYERS * rim_rows :], "sp", 1)
    current = jnp.concatenate([earlier, stream], axis=0)
    for layer_index in range(LAYERS):
        prefix = (LAYERS - layer_index) * rim_rows
        gathered = lax.all_gather(current, "tp", axis=1, tiled=True)
        gathered32 = gathered.astype(jnp.float32)
        scale = lax.rsqrt(jnp.sum(gathered32 * gathered32, axis=1, keepdims=True) / D + EPS)
        run_normed = (gathered32 * scale * norm_gain[layer_index]).astype(jnp.bfloat16)
        value_proj = jnp.dot(
            run_normed, value_all[:, layer_index], preferred_element_type=jnp.float32
        )
        gate_proj = jnp.dot(
            run_normed, gate_all[:, layer_index], preferred_element_type=jnp.float32
        )
        glu_out = value_proj * jax.nn.sigmoid(gate_proj)
        positions = (
            lax.axis_index("sp") * tokens_here - prefix + lax.iota(jnp.int32, current.shape[0])
        )
        extended = jnp.where((positions >= 0)[:, None], glu_out, 0.0)
        residual = current[rim_rows:].astype(jnp.float32)
        conv_out = valid_conv(extended, my_taps[layer_index])
        first_sums, square_sums = lax.psum(
            (jnp.sum(conv_out, axis=1), jnp.sum(conv_out * conv_out, axis=1)), "tp"
        )
        row_mean = (first_sums / C)[:, None]
        row_var = (square_sums / C)[:, None] - row_mean * row_mean
        run_active = jax.nn.silu(
            (conv_out - row_mean) * lax.rsqrt(row_var + EPS) * my_ln_gain[layer_index]
            + my_ln_bias[layer_index]
        ).astype(jnp.bfloat16)
        partial_value = jnp.dot(
            run_active, out_all[:, :, layer_index], preferred_element_type=jnp.float32
        )
        summed = lax.psum_scatter(
            partial_value.astype(jnp.bfloat16), "tp", scatter_dimension=1, tiled=True
        ).astype(jnp.float32)
        current = (residual + summed).astype(jnp.bfloat16)
    final32 = current.astype(jnp.float32)
    squares = lax.psum(jnp.sum(final32 * final32, axis=1), "tp")
    return (final32 * lax.rsqrt(squares[:, None] / D + EPS) * my_final).astype(jnp.bfloat16)


def solution(mesh):
    placed = (P("sp", "tp"), P(), P("sp", "tp"), P("sp", "tp"), P(), P(), P(), P("tp", "sp"), P())
    return jax.shard_map(
        local, mesh=mesh, in_specs=placed, out_specs=P("sp", "tp"), check_vma=False
    )
```

profile of v0, /device:TPU:8, one launch (start us, length us, event | category | flops | bytes accessed | tf_op | source)
XLA Modules:
  0.0 276.4 jit_solution(3715247902081535697)
XLA Ops:
  9.7 1.9 collective-permute-start
  17.9 12.1 %all_gather.15 = bf16[188,2048]{1,0:T(8,128)(2,1)S(1)} all-gather(bf16[188,1024]{1,0:T(8,128)(2,1)S(1)} %pad_maximum_fusion), channel_id=1, replica_groups=mesh['sp'=16,'tp'=2] {'tp'}, dimensions={1}, use_global_device_ids=true | all-gather | bytes 1155072 | tf_op jit(solution)/shard_map/all_gather | solution.py:61
  30.3 30.8 %all-gather.6.cloned.1.call-done = bf16[4096,512]{1,0:T(8,128)(2,1)} async-done(((bf16[256,512]{1,0:T(8,128)(2,1)}), bf16[4096,512]{1,0:T(8,128)(2,1)}) %all-gather.6.cloned.1.call-update) | async-done | bytes 4194320 | tf_op jit(solution)/shard_map/all_gather | solution.py:51
  61.1 7.2 %reshape.177 = bf16[2048,2,512]{2,1,0:T(2,128)(2,1)} reshape(bf16[4096,512]{1,0:T(8,128)(2,1)} %all-gather.6.cloned.1.call-done) | data formatting | bytes 8388608 | tf_op jit(solution)/shard_map/reshape | solution.py:55
  68.3 43.9 %all-gather.4.cloned.1.call-done = bf16[4096,512]{1,0:T(8,128)(2,1)} async-done(((bf16[256,512]{1,0:T(8,128)(2,1)}), bf16[4096,512]{1,0:T(8,128)(2,1)}) %all-gather.4.cloned.1.call-update) | async-done | bytes 4194320 | tf_op jit(solution)/shard_map/all_gather | solution.py:50
  112.2 7.2 %reshape.176 = bf16[2048,2,512]{2,1,0:T(2,128)(2,1)} reshape(bf16[4096,512]{1,0:T(8,128)(2,1)} %all-gather.4.cloned.1.call-done) | data formatting | bytes 8388608 | tf_op jit(solution)/shard_map/reshape | solution.py:54
  119.4 10.0 %fusion.141 = (bf16[2048,1,512]{2,1,0:T(2,128)(2,1)}, bf16[2048,1,512]{2,1,0:T(2,128)(2,1)}) fusion(bf16[2048,2,512]{2,1,0:T(2,128)(2,1)} %reshape.177), kind=kLoop, calls=%fused_computation.233 | loop fusion | bytes 8388608 | tf_op jit(solution)/shard_map/slice | solution.py:69
  129.4 7.0 %fusion.140 = (bf16[2048,1,512]{2,1,0:T(2,128)(2,1)}, bf16[2048,1,512]{2,1,0:T(2,128)(2,1)}) fusion(bf16[2048,2,512]{2,1,0:T(2,128)(2,1)S(1)} %copy-done), kind=kLoop, calls=%fused_computation.232 | loop fusion | bytes 8388608 | tf_op jit(solution)/shard_map/slice | solution.py:66
  136.4 27.2 %all-gather.8.cloned.1.call-done = bf16[512,4096]{1,0:T(8,128)(2,1)} async-done(((bf16[512,256]{1,0:T(8,128)(2,1)}), bf16[512,4096]{1,0:T(8,128)(2,1)}) %all-gather.8.cloned.1.call-update) | async-done | bytes 4194320 | tf_op jit(solution)/shard_map/all_gather | solution.py:52
  163.6 6.5 %copy.13 = bf16[512,4096]{0,1:T(8,128)(2,1)} copy(bf16[512,4096]{1,0:T(8,128)(2,1)} %all-gather.8.cloned.1.call-done) | data formatting | bytes 8388608 | tf_op jit(solution)/shard_map/all_gather | solution.py:52
  170.1 7.2 %reshape.178 = bf16[512,2048,2]{0,2,1:T(2,128)(2,1)} reshape(bf16[512,4096]{0,1:T(8,128)(2,1)} %copy.13) | data formatting | bytes 8388608 | tf_op jit(solution)/shard_map/reshape | solution.py:56
  177.3 9.9 %fusion.142 = (bf16[512,2048,1]{0,2,1:T(2,128)(2,1)}, bf16[512,2048,1]{0,2,1:T(2,128)(2,1)}) fusion(bf16[512,2048,2]{0,2,1:T(2,128)(2,1)} %reshape.178), kind=kLoop, calls=%fused_computation.234 | loop fusion | bytes 8388608 | tf_op jit(solution)/shard_map/slice | solution.py:88
  187.3 9.0 %copy.14 = bf16[512,2048,1]{1,0,2:T(8,128)(2,1)S(1)} copy(bf16[512,2048,1]{0,2,1:T(2,128)(2,1)} %get-tuple-element.19) | data formatting | bytes 4194304 | tf_op jit(solution)/shard_map/slice | solution.py:88
  196.3 3.0 %fusion.29 = f32[188,512]{1,0:T(8,128)S(1)} fusion(bf16[2048,1,512]{2,1,0:T(2,128)(2,1)} %get-tuple-element.17, bf16[188,2048]{1,0:T(8,128)(2,1)S(1)} %all_gather.15, f32[2048]{0:T(1024)S(1)} %bitcast.145, f32[188]{0:T(256)S(1)} %add_rsqrt_fusion.2), kind=kOutput, calls=%fused_computation.29 | convolution fusion | flops 396093440 | bytes 3261168 | tf_op jit(solution)/shard_map/dot_general | solution.py:68
  201.8 4.9 %all-reduce.1 = (f32[158]{0:T(256)S(1)}, f32[158]{0:T(256)S(1)}) all-reduce(f32[158]{0:T(256)S(1)} %get-tuple-element.6, f32[158]{0:T(256)S(1)} %get-tuple-element.5), channel_id=1, replica_groups=mesh['sp'=16,'tp'=2] {'tp'}, use_global_device_ids=true, to_apply=%region_4.5 | all-reduce | flops 316 | bytes 2528 | tf_op jit(solution)/shard_map/psum | solution.py:78
  206.8 1.5 convolution_convert_fusion
  208.4 9.1 %copy.15 = bf16[512,2048,1]{1,0,2:T(8,128)(2,1)S(1)} copy(bf16[512,2048,1]{0,2,1:T(2,128)(2,1)} %get-tuple-element.20) | data formatting | bytes 4194304 | tf_op jit(solution)/shard_map/slice | solution.py:88
  217.5 7.0 %reduce-scatter.3.cloned.1.call-done = bf16[158,1024]{1,0:T(8,128)(2,1)} async-done(((bf16[158,2048]{1,0:T(8,128)(2,1)}), bf16[158,1024]{1,0:T(8,128)(2,1)}) %reduce-scatter.3.cloned.1.call-update) | async-done | bytes 323600 | tf_op jit(solution)/shard_map/reduce_scatter | solution.py:90
  225.5 9.9 %all_gather.19 = bf16[158,2048]{1,0:T(8,128)(2,1)S(1)} all-gather(bf16[158,1024]{1,0:T(8,128)(2,1)S(1)} %add_convert_fusion), channel_id=1, replica_groups=mesh['sp'=16,'tp'=2] {'tp'}, dimensions={1}, use_global_device_ids=true | all-gather | bytes 970752 | tf_op jit(solution)/shard_map/all_gather | solution.py:61
  235.7 3.0 %fusion.50 = f32[158,512]{1,0:T(8,128)S(1)} fusion(bf16[2048,1,512]{2,1,0:T(2,128)(2,1)} %get-tuple-element.18, bf16[158,2048]{1,0:T(8,128)(2,1)S(1)} %all_gather.19, f32[2048]{0:T(1024)S(1)} %bitcast.143, f32[158]{0:T(256)S(1)} %add_rsqrt_fusion), kind=kOutput, calls=%fused_computation.36 | convolution fusion | flops 332887040 | bytes 3076728 | tf_op jit(solution)/shard_map/dot_general | solution.py:68
  240.9 4.9 %all-reduce = (f32[128]{0:T(128)S(1)}, f32[128]{0:T(128)S(1)}) all-reduce(f32[128]{0:T(128)S(1)} %get-tuple-element.8, f32[128]{0:T(128)S(1)} %get-tuple-element.7), channel_id=1, replica_groups=mesh['sp'=16,'tp'=2] {'tp'}, use_global_device_ids=true, to_apply=%region_10.11 | all-reduce | flops 256 | bytes 2048 | tf_op jit(solution)/shard_map/psum | solution.py:78
  247.2 14.8 %reduce-scatter.5.cloned.1.call-done = bf16[128,1024]{1,0:T(8,128)(2,1)} async-done(((bf16[128,2048]{1,0:T(8,128)(2,1)}), bf16[128,1024]{1,0:T(8,128)(2,1)}) %reduce-scatter.5.cloned.1.call-update) | async-done | bytes 262160 | tf_op jit(solution)/shard_map/reduce_scatter | solution.py:90
  263.1 4.9 %psum.39 = f32[128]{0:T(128)S(1)} all-reduce(f32[128]{0:T(128)S(1)} %fusion.56), channel_id=1, replica_groups=mesh['sp'=16,'tp'=2] {'tp'}, use_global_device_ids=true, to_apply=%region_13.14 | all-reduce | flops 128 | bytes 1024 | tf_op jit(solution)/shard_map/psum | solution.py:95
  268.1 1.8 fusion.58
  (44 shorter events, 18.3 us)
Async XLA Ops:
  6.5 54.6 %all-gather.6.cloned.1.call-start = ((), (), s32[]{:S(2)}) async-start(), calls=%async_computation.3 | async-start | bytes 4456448 | tf_op jit(solution)/shard_map/all_gather | solution.py:51
  7.3 104.9 %all-gather.4.cloned.1.call-start = ((), (), s32[]{:S(2)}) async-start(), calls=%async_computation.2 | async-start | bytes 4456448 | tf_op jit(solution)/shard_map/all_gather | solution.py:50
  8.0 155.6 %all-gather.8.cloned.1.call-start = ((), (), s32[]{:S(2)}) async-start(), calls=%async_computation.4 | async-start | bytes 4456448 | tf_op jit(solution)/shard_map/all_gather | solution.py:52
  8.7 215.7 %reduce-scatter.3.cloned.1.call-start = ((), (), s32[]{:S(2)}) async-start(), calls=%async_computation.5 | async-start | bytes 983040 | tf_op jit(solution)/shard_map/reduce_scatter | solution.py:90
  9.7 7.2 %collective-permute-start = (bf16[60,1024]{1,0:T(8,128)(2,1)S(1)}, bf16[60,1024]{1,0:T(8,128)(2,1)S(1)}, u32[]{:S(2)}, u32[]{:S(2)}) collective-permute-start(bf16[60,1024]{1,0:T(8,128)(2,1)S(1)} %slice.543), channel_id=1, source_target_pairs={{0,2},{2,4},{4,6},{6,8},{8,10},{10,12},{12,14},{14,16},{16,18},{18... | collective-permute-start | bytes 368648 | tf_op jit(solution)/shard_map/ppermute | solution.py:18
  119.4 10.0 %copy-start = (bf16[2048,2,512]{2,1,0:T(2,128)(2,1)S(1)}, bf16[2048,2,512]{2,1,0:T(2,128)(2,1)}, u32[]{:S(2)}) copy-start(bf16[2048,2,512]{2,1,0:T(2,128)(2,1)} %reshape.176) | copy-start | bytes 12582916
  196.2 3.5 %copy-start.2 = (bf16[2048,1,512]{2,1,0:T(2,128)(2,1)S(1)}, bf16[2048,1,512]{2,1,0:T(2,128)(2,1)}, u32[]{:S(2)}) copy-start(bf16[2048,1,512]{2,1,0:T(2,128)(2,1)} %get-tuple-element.16) | copy-start | bytes 6291460
  208.3 53.7 %reduce-scatter.5.cloned.1.call-start = ((), (), s32[]{:S(2)}) async-start(), calls=%async_computation.6 | async-start | bytes 786432 | tf_op jit(solution)/shard_map/reduce_scatter | solution.py:90
  208.4 16.1 %copy-start.3 = (bf16[128,1024]{1,0:T(8,128)(2,1)S(1)}, bf16[128,1024]{1,0:T(8,128)(2,1)}, u32[]{:S(2)}) copy-start(bf16[128,1024]{1,0:T(8,128)(2,1)} %param.9) | copy-start | bytes 786436
  235.7 3.5 %copy-start.1 = (bf16[2048,1,512]{2,1,0:T(2,128)(2,1)S(1)}, bf16[2048,1,512]{2,1,0:T(2,128)(2,1)}, u32[]{:S(2)}) copy-start(bf16[2048,1,512]{2,1,0:T(2,128)(2,1)} %get-tuple-element.15) | copy-start | bytes 6291460
  240.9 6.3 %copy-start.4 = (f32[2048]{0:T(1024)S(1)}, f32[2048]{0:T(1024)}, u32[]{:S(2)}) copy-start(f32[2048]{0:T(1024)} %param.17) | copy-start | bytes 24580
Sparse Core Ops, SparseCore 0:
  9.5 51.5 all-gather.5
  63.3 48.8 all-gather.3
  114.4 49.2 all-gather.7
  208.4 15.9 reduce-scatter.2
  247.3 14.6 reduce-scatter.4
where the time goes:
time: 279 us; the launch traced here: 276 us
  waiting for transfers between devices  127 us (46%)
  local copies, waits for them, and re-layouts  78.9 us (28%)
  blocking collectives  36.8 us (13%)
  between operations  13.3 us (5%)
  matrix products  10 us (4%)
  other arithmetic  8.24 us (3%)
    all_gather x1, waiting for transfers between devices, local(): lax.all_gather(value_weight, 'sp', axis=0, tiled=True)  43.9 us
    all_gather x1, waiting for transfers between devices, local(): lax.all_gather(gate_weight, 'sp', axis=0, tiled=True)  30.8 us
    slice x3, local copies, waits for them, and re-layouts, local(): out_all[:, :, layer_index]  28 us
    all_gather x1, waiting for transfers between devices, local(): lax.all_gather(out_weight, 'sp', axis=1, tiled=True)  27.2 us
    all_gather x2, blocking collectives, local(): gathered = lax.all_gather(current, 'tp', axis=1, tiled=True)  22 us
    reduce_scatter x2, waiting for transfers between devices, local(): lax.psum_scatter(partial_value.astype(jnp.bfloat16), 'tp', scatter_dimens...  21.7 us
    slice x1, local copies, waits for them, and re-layouts, local(): gate_all[:, layer_index]  9.98 us
    psum x2, blocking collectives, local(): lax.psum((jnp.sum(conv_out, axis=1), jnp.sum(conv_out * conv_out, axis=1)...  9.87 us
  transfers between devices with their start and end apart: 6, of which 6 were waited for; matrix products, arithmetic and copies ran while one was open for 17% of the time, Pallas kernels for 0%

commit v1 on v0

--- a/solution.py
+++ b/solution.py
@@ -1,6 +1,10 @@
+import functools
+
 import jax
 import jax.numpy as jnp
 from jax import lax
+from jax.experimental import pallas as pl
+from jax.experimental.pallas import tpu as pltpu
 from jax.sharding import PartitionSpec as P
 
 D = 2048
@@ -96,8 +100,339 @@
     return (final32 * lax.rsqrt(squares[:, None] / D + EPS) * my_final).astype(jnp.bfloat16)
 
 
+MESH = pl.DeviceIdType.MESH
+HALO = 32
+UP, DOWN, SIDE, CORE = range(4)
+ITEMS = 3 * LAYERS
+
+
+def fused_kernel(
+    n, x_ref, ng_ref, v_ref, g_ref, taps_ref, lng_ref, lnb_ref, o_ref, fg_ref, out_ref,
+    vg, ob, xf, xn, nb, ext, cv, act, part, rpart, st, rst,
+    ssem, rsem, xsem, hsem, tsem, psem,
+):
+    levels = n // 4
+    sp = lax.axis_index("sp")
+    tp = lax.axis_index("tp")
+    z, y, core = sp // 4, (sp // 2) % 2, sp % 2
+    peer = 1 - tp
+    rows, cols = x_ref.shape
+    depth = v_ref.shape[0] // LAYERS
+    ch = v_ref.shape[1]
+    width = o_ref.shape[1] // LAYERS
+    has_up, has_down = z < levels - 1, z > 0
+    target = {UP: sp + 4, DOWN: sp - 4, SIDE: sp + 2 - 4 * y, CORE: sp + 1 - 2 * core}
+
+    def slot(k, src):
+        layer, kind = divmod(k, 3)
+        return ob.at[layer, src] if kind == 2 else vg.at[layer * 2 + kind, src]
+
+    def copy(k, src, way):
+        return pltpu.make_async_remote_copy(
+            src_ref=slot(k, src), dst_ref=slot(k, src),
+            send_sem=ssem.at[k, way, src], recv_sem=rsem.at[k, src],
+            device_id={"sp": target[way], "tp": tp}, device_id_type=MESH)
+
+    def index(zz, yy, cc):
+        return (zz * 2 + yy) * 2 + cc
+
+    def from_below(d):
+        return index(z - d, y, core)
+
+    def from_above(d):
+        return index(z + d, y, core)
+
+    def own(k, act_on):
+        act_on(k, sp, SIDE)
+        pl.when(has_up)(lambda: act_on(k, sp, UP))
+        pl.when(has_down)(lambda: act_on(k, sp, DOWN))
+        act_on(k, sp, CORE)
+
+    def line(k, act_on, wait):
+        for d in range(1, levels):
+            @pl.when(z - d >= 0)
+            def _():
+                if wait:
+                    copy(k, from_below(d), UP).wait_recv()
+                act_on(k, from_below(d), SIDE)
+                pl.when(has_up)(lambda: act_on(k, from_below(d), UP))
+                act_on(k, from_below(d), CORE)
+
+            @pl.when(z + d < levels)
+            def _():
+                if wait:
+                    copy(k, from_above(d), DOWN).wait_recv()
+                act_on(k, from_above(d), SIDE)
+                pl.when(has_down)(lambda: act_on(k, from_above(d), DOWN))
+                act_on(k, from_above(d), CORE)
+
+    def across(k, act_on, wait):
+        def one(src):
+            if wait:
+                copy(k, src, SIDE).wait_recv()
+            act_on(k, src, CORE)
+
+        one(index(z, 1 - y, core))
+        for d in range(1, levels):
+            pl.when(z - d >= 0)(lambda: one(index(z - d, 1 - y, core)))
+            pl.when(z + d < levels)(lambda: one(index(z + d, 1 - y, core)))
+
+    def other_core(k):
+        for zz in range(levels):
+            for yy in range(2):
+                copy(k, index(zz, yy, 1 - core), CORE).wait_recv()
+
+    def start(k, src, way):
+        copy(k, src, way).start()
+
+    def finish(k, src, way):
+        copy(k, src, way).wait_send()
+
+    def to_peer(src, dst, sems):
+        return pltpu.make_async_remote_copy(
+            src_ref=src, dst_ref=dst, send_sem=sems[0], recv_sem=sems[1],
+            device_id={"sp": sp, "tp": peer}, device_id_type=MESH)
+
+    def halo(layer):
+        return pltpu.make_async_remote_copy(
+            src_ref=ext.at[layer, pl.ds(rows, HALO)], dst_ref=ext.at[layer, pl.ds(0, HALO)],
+            send_sem=hsem.at[layer, 0], recv_sem=hsem.at[layer, 1],
+            device_id={"sp": sp + 1, "tp": tp}, device_id_type=MESH)
+
+    barrier = pltpu.get_barrier_semaphore()
+
+    def greet(device):
+        pl.semaphore_signal(barrier, inc=1, device_id=device, device_id_type=MESH)
+
+    greet({"sp": target[SIDE], "tp": tp})
+    greet({"sp": target[CORE], "tp": tp})
+    greet({"sp": sp, "tp": peer})
+    pl.when(has_up)(lambda: greet({"sp": target[UP], "tp": tp}))
+    pl.when(has_down)(lambda: greet({"sp": target[DOWN], "tp": tp}))
+    pl.when(sp < n - 1)(lambda: greet({"sp": sp + 1, "tp": tp}))
+    pl.when(sp > 0)(lambda: greet({"sp": sp - 1, "tp": tp}))
+
+    lo = lax.broadcasted_iota(jnp.int32, (depth, LAYERS * depth), 0)
+    hi = lax.broadcasted_iota(jnp.int32, (depth, LAYERS * depth), 1)
+    clo = lax.broadcasted_iota(jnp.int32, (LAYERS * width, width), 1)
+    chi = lax.broadcasted_iota(jnp.int32, (LAYERS * width, width), 0)
+
+    for layer in range(LAYERS):
+        pick = (hi == LAYERS * lo + layer).astype(jnp.float32).astype(jnp.bfloat16)
+        for kind, ref in enumerate((v_ref, g_ref)):
+            vg[layer * 2 + kind, sp] = jnp.dot(
+                pick, ref[...], preferred_element_type=jnp.float32).astype(jnp.bfloat16)
+        pick = (chi == LAYERS * clo + layer).astype(jnp.float32).astype(jnp.bfloat16)
+        ob[layer, sp] = jnp.dot(
+            o_ref[...], pick, preferred_element_type=jnp.float32).astype(jnp.bfloat16)
+    xf[tp] = x_ref[...]
+
+    @pl.when(sp == 0)
+    def _():
+        for layer in range(LAYERS):
+            ext[layer, 0:HALO] = jnp.zeros((HALO, ch), jnp.float32)
+
+    ends = [has_up, has_down, sp < n - 1, sp > 0]
+    pl.semaphore_wait(barrier, 3 + sum(end.astype(jnp.int32) for end in ends))
+
+    own(0, start)
+    x_copy = to_peer(x_ref, xf.at[tp], (xsem.at[0], xsem.at[1]))
+    x_copy.start()
+    own(1, start)
+
+    def normalise(source, layer):
+        total = jnp.zeros((rows, 1), jnp.float32)
+        for half in range(2):
+            value = source[half].astype(jnp.float32)
+            total = total + jnp.sum(value * value, axis=1, keepdims=True)
+        scale = lax.rsqrt(total / D + EPS)
+        for half in range(2):
+            value = source[half].astype(jnp.float32)
+            gain = ng_ref[layer : layer + 1, half * cols : (half + 1) * cols]
+            nb[:, half * cols : (half + 1) * cols] = (value * scale * gain).astype(jnp.bfloat16)
+
+    def glu(layer):
+        value, gate = (
+            jnp.dot(nb[...], vg[layer * 2 + kind].reshape(n * depth, ch),
+                    preferred_element_type=jnp.float32) for kind in range(2))
+        ext[layer, HALO:] = value * jax.nn.sigmoid(gate)
+        pl.when(sp < n - 1)(lambda: halo(layer).start())
+
+    def stat_copy(i):
+        return to_peer(st.at[i], rst.at[i], (tsem.at[i, 0], tsem.at[i, 1]))
+
+    def send_stats(i, first, second):
+        lane = lax.broadcasted_iota(jnp.int32, (rows, 128), 1)
+        turned = jnp.where(lane < 64, first, second).T
+        st[i, 0:8] = turned[0:8]
+        st[i, 8:16] = turned[64:72]
+        stat_copy(i).start()
+
+    def take_stats(i):
+        stat_copy(i).wait_recv()
+        both = st[i] + rst[i]
+        turned = jnp.concatenate([both] * (128 // 16), axis=0).T
+        return turned[:, 0:1], turned[:, 8:9]
+
+    def conv(layer):
+        tap_cols = pl.ds(pl.multiple_of(tp * ch, 128), ch)
+
+        def chunk(r0):
+            running = jnp.zeros((HALO, ch), jnp.float32)
+            for k in range(KW):
+                at = r0 + k + HALO - (KW - 1)
+                running = running + taps_ref[layer, k : k + 1, tap_cols] * ext[layer, at : at + HALO]
+            cv[r0 : r0 + HALO] = running
+
+        for r0 in range(HALO, rows, HALO):
+            chunk(r0)
+        pl.when(sp > 0)(lambda: halo(layer).wait_recv())
+        chunk(0)
+        value = cv[...]
+        send_stats(layer, jnp.sum(value, axis=1, keepdims=True),
+                   jnp.sum(value * value, axis=1, keepdims=True))
+
+    def activate(layer):
+        first, second = take_stats(layer)
+        mean = first / C
+        var = second / C - mean * mean
+        here = pl.ds(pl.multiple_of(tp * ch, 128), ch)
+        v = (cv[...] - mean) * lax.rsqrt(var + EPS) * lng_ref[layer : layer + 1, here]
+        v = v + lnb_ref[layer : layer + 1, here]
+        act[...] = (v / (1.0 + jnp.exp(-v))).astype(jnp.bfloat16)
+
+    pairs = n // 2
+    half_pairs = pairs // 2
+
+    def part_copy(layer, p):
+        return to_peer(part.at[layer, p], rpart.at[layer, p], (psem.at[layer, 0, p], psem.at[layer, 1, p]))
+
+    def project(layer, p):
+        weights = jnp.concatenate([ob[layer, 2 * p], ob[layer, 2 * p + 1]], axis=1)
+        part[layer, p] = jnp.dot(
+            act[...], weights, preferred_element_type=jnp.float32).astype(jnp.bfloat16)
+
+    def add_parts(layer, p):
+        return part[layer, p].astype(jnp.float32) + rpart[layer, p].astype(jnp.float32)
+
+    own(2, start)
+    line(0, start, True)
+    x_copy.wait_recv()
+    normalise(xf, 0)
+    own(3, start)
+    line(1, start, True)
+    across(0, start, True)
+    own(4, start)
+    line(2, start, True)
+    across(1, start, True)
+    own(5, start)
+    other_core(0)
+    other_core(1)
+    glu(0)
+    line(3, start, True)
+    conv(0)
+    across(2, start, True)
+    activate(0)
+    other_core(2)
+    for p in range(pairs):
+        project(0, p)
+        part_copy(0, p).start()
+    line(4, start, True)
+    across(3, start, True)
+    for p in range(pairs):
+        part_copy(0, p).wait_recv()
+        half, at = p // half_pairs, (p % half_pairs) * 2 * width
+        here = xf[half, :, at : at + 2 * width].astype(jnp.float32)
+        xn[half, :, at : at + 2 * width] = (here + add_parts(0, p)).astype(jnp.bfloat16)
+    normalise(xn, 1)
+    line(5, start, True)
+    across(4, start, True)
+    other_core(3)
+    other_core(4)
+    glu(1)
+    conv(1)
+    across(5, start, True)
+    activate(1)
+    other_core(5)
+    for q in range(half_pairs):
+        project(1, peer * half_pairs + q)
+        part_copy(1, peer * half_pairs + q).start()
+    for q in range(half_pairs):
+        project(1, tp * half_pairs + q)
+    squares = jnp.zeros((rows, 1), jnp.float32)
+    for q in range(half_pairs):
+        p = tp * half_pairs + q
+        part_copy(1, p).wait_recv()
+        at = q * 2 * width
+        here = xn[tp, :, at : at + 2 * width].astype(jnp.float32)
+        fresh = (here + add_parts(1, p)).astype(jnp.bfloat16)
+        out_ref[:, at : at + 2 * width] = fresh
+        fresh = fresh.astype(jnp.float32)
+        squares = squares + jnp.sum(fresh * fresh, axis=1, keepdims=True)
+    send_stats(LAYERS, squares, squares)
+    total, _ = take_stats(LAYERS)
+    gain = fg_ref[0:1, pl.ds(pl.multiple_of(tp * cols, 128), cols)]
+    out_ref[...] = (
+        out_ref[...].astype(jnp.float32) * lax.rsqrt(total / D + EPS) * gain).astype(jnp.bfloat16)
+
+    for k in range(ITEMS):
+        own(k, finish)
+        line(k, finish, False)
+        across(k, finish, False)
+    x_copy.wait_send()
+    for layer in range(LAYERS):
+        pl.when(sp < n - 1)(lambda: halo(layer).wait_send())
+    for i in range(LAYERS + 1):
+        stat_copy(i).wait_send()
+    for p in range(pairs):
+        part_copy(0, p).wait_send()
+    for q in range(half_pairs):
+        part_copy(1, peer * half_pairs + q).wait_send()
+
+
+def fused(n, stream, norm_gain, value_weight, gate_weight, conv_taps, ln_gain, ln_bias, out_weight, final_gain):
+    rows, cols = stream.shape
+    depth, ch = value_weight.shape[0] // LAYERS, value_weight.shape[1]
+    width = out_weight.shape[1] // LAYERS
+    bf16, f32 = jnp.bfloat16, jnp.float32
+    dma = pltpu.SemaphoreType.DMA
+    return pl.pallas_call(
+        functools.partial(fused_kernel, n),
+        out_shape=jax.ShapeDtypeStruct((rows, cols), bf16),
+        in_specs=[pl.BlockSpec(memory_space=pltpu.VMEM)] * 9,
+        out_specs=pl.BlockSpec(memory_space=pltpu.VMEM),
+        scratch_shapes=[
+            pltpu.VMEM((2 * LAYERS, n, depth, ch), bf16),
+            pltpu.VMEM((LAYERS, n, ch, width), bf16),
+            pltpu.VMEM((2, rows, cols), bf16),
+            pltpu.VMEM((2, rows, cols), bf16),
+            pltpu.VMEM((rows, 2 * cols), bf16),
+            pltpu.VMEM((LAYERS, HALO + rows, ch), f32),
+            pltpu.VMEM((rows, ch), f32),
+            pltpu.VMEM((rows, ch), bf16),
+            pltpu.VMEM((LAYERS, n // 2, rows, 2 * width), bf16),
+            pltpu.VMEM((LAYERS, n // 2, rows, 2 * width), bf16),
+            pltpu.VMEM((LAYERS + 1, 16, rows), f32),
+            pltpu.VMEM((LAYERS + 1, 16, rows), f32),
+            dma((ITEMS, 4, n)),
+            dma((ITEMS, n)),
+            dma((2,)),
+            dma((LAYERS, 2)),
+            dma((LAYERS + 1, 2)),
+            dma((LAYERS, 2, n // 2)),
+        ],
+        compiler_params=pltpu.CompilerParams(collective_id=0, has_side_effects=True),
+    )(stream, norm_gain, value_weight, gate_weight, conv_taps, ln_gain, ln_bias, out_weight,
+      final_gain.reshape(1, -1))
+
+
 def solution(mesh):
     placed = (P("sp", "tp"), P(), P("sp", "tp"), P("sp", "tp"), P(), P(), P(), P("tp", "sp"), P())
-    return jax.shard_map(
-        local, mesh=mesh, in_specs=placed, out_specs=P("sp", "tp"), check_vma=False
-    )
+    n, n_tp = mesh.shape["sp"], mesh.shape["tp"]
+
+    def step(*args):
+        stream, out_weight = args[0], args[7]
+        fits = n_tp == 2 and n % 4 == 0 and stream.shape[0] == 128 and out_weight.shape[1] == 128 * LAYERS
+        return fused(n, *args) if fits else local(*args)
+
+    return jax.shard_map(step, mesh=mesh, in_specs=placed, out_specs=P("sp", "tp"), check_vma=False)

time: 279 us -> 101 us (0.36)
  waiting for transfers between devices: 127 us -> 0 us
  Pallas kernels: 0 us -> 97.4 us
  local copies, waits for them, and re-layouts: 78.9 us -> 3.41 us
  blocking collectives: 36.8 us -> 0 us
  between operations: 13.3 us -> 0.01 us
  matrix products: 10 us -> 0 us
  other arithmetic: 8.24 us -> 0 us
    all_gather x3 -> x0, waiting for transfers between devices: 102 us -> none  [the longest x1 43.9 us: local(): lax.all_gather(value_weight, 'sp', axis=0, tiled=True)]
    pallas_call x0 -> x1, Pallas kernels: none -> 97.4 us  [fused(): pl.pallas_call(functools.partial(fused_kernel, n), out_shape=jax.ShapeDty...]
    slice x10 -> x0, local copies, waits for them, and re-layouts: 49.9 us -> none  [the longest x3 28 us: local(): out_all[:, :, layer_index]]
    all_gather x2 -> x0, blocking collectives: 22 us -> none  [local(): gathered = lax.all_gather(current, 'tp', axis=1, tiled=True)]
    reduce_scatter x2 -> x0, waiting for transfers between devices: 21.7 us -> none  [local(): lax.psum_scatter(partial_value.astype(jnp.bfloat16), 'tp', scatter_dimens...]
    reshape x3 -> x0, local copies, waits for them, and re-layouts: 21.6 us -> none  [the longest x1 7.22 us: local(): value_all = value_all.reshape(D, LAYERS, channels)]
    psum x3 -> x0, blocking collectives: 14.8 us -> none  [the longest x2 9.87 us: local(): lax.psum((jnp.sum(conv_out, axis=1), jnp.sum(conv_out * conv_out, axis=1)...]
    dot_general x6 -> x0, matrix products: 10 us -> none  [the longest x2 5.99 us: local(): jnp.dot(run_normed, gate_all[:, layer_index], preferred_element_type=jnp....]
  transfers between devices with their start and end apart: 6 -> 0, of which waited for: 6 -> 0; matrix products, arithmetic and copies ran while one was open for 17% -> 0% of each run, Pallas kernels for 0% -> 0%
where the time goes in v1:
time: 101 us
  Pallas kernels  97.4 us (96%)
  local copies, waits for them, and re-layouts  3.41 us (3%)
    pallas_call x1, Pallas kernels, fused(): pl.pallas_call(functools.partial(fused_kernel, n), out_shape=jax.ShapeDty...  97.4 us
    unnamed x2, local copies, waits for them, and re-layouts  3.41 us

profile of v1, /device:TPU:8, one launch (start us, length us, event | category | flops | bytes accessed | tf_op | source)
XLA Modules:
  0.0 100.8 jit_solution(5891114074840092279)
XLA Ops:
  0.0 1.7 %copy.10.taps_ref = f32[2,31,1024]{2,1,0:T(8,128)} copy(f32[2,31,1024]{2,0,1:T(2,128)} %param.13) | data formatting | bytes 507904 | tf_op args[4]
  1.7 97.4 %shard_map.91 = bf16[128,1024]{1,0:T(8,128)(2,1)} custom-call(bf16[128,1024]{1,0:T(8,128)(2,1)} %x_ref.1, f32[2,2048]{1,0:T(2,128)} %ng_ref.1, bf16[256,512]{1,0:T(8,128)(2,1)} %v_ref.1, bf16[256,512]{1,0:T(8,128)(2,1)} %g_ref.1, f32[2,31,1024]{2,1,0:T(8,128)} %copy.10.taps_ref, f32[2,1024]{1,0:T(2,128)} %lng_ref.1, f32[2,1024]{1,0:T(2,128)} %lnb_ref.1, ...), custom_call_target="tpu_custom_call" | custom-call | tf_op jit(solution)/shard_map/pallas_call | solution.py:399
  99.1 1.7 %copy.12 = bf16[128,1024]{1,0:T(8,128)(2,1)} copy(bf16[128,1024]{1,0:T(8,128)(2,1)} %shard_map.91) | data formatting | bytes 524288

commit v2 on v1

--- a/solution.py
+++ b/solution.py
@@ -104,13 +104,22 @@
 HALO = 32
 UP, DOWN, SIDE, CORE = range(4)
 ITEMS = 3 * LAYERS
+PAIRED = (0, 2, 4)
 
 
 def fused_kernel(
-    n, x_ref, ng_ref, v_ref, g_ref, taps_ref, lng_ref, lnb_ref, o_ref, fg_ref, out_ref,
-    vg, ob, xf, xn, nb, ext, cv, act, part, rpart, st, rst,
+    n, x_in, ng_in, v_in, g_in, taps_in, lng_in, lnb_in, o_in, fg_in, out_ref,
+    x_ref, ng_ref, v_ref, g_ref, taps_ref, lng_ref, lnb_ref, o_ref, fg_ref, isem, vg, ob, xf, xn, nb, ext, cv, act, part, rpart, st, rst,
     ssem, rsem, xsem, hsem, tsem, psem,
 ):
+    loads = [
+        pltpu.make_async_copy(source, to, isem.at[i])
+        for i, (source, to) in enumerate((
+            (v_in, v_ref), (g_in, g_ref), (x_in, x_ref), (o_in, o_ref), (ng_in, ng_ref),
+            (taps_in, taps_ref), (lng_in, lng_ref), (lnb_in, lnb_ref), (fg_in, fg_ref)))
+    ]
+    for load in loads:
+        load.start()
     levels = n // 4
     sp = lax.axis_index("sp")
     tp = lax.axis_index("tp")
@@ -121,6 +130,7 @@
     ch = v_ref.shape[1]
     width = o_ref.shape[1] // LAYERS
     has_up, has_down = z < levels - 1, z > 0
+    even, odd = z % 2 == 0, z % 2 == 1
     target = {UP: sp + 4, DOWN: sp - 4, SIDE: sp + 2 - 4 * y, CORE: sp + 1 - 2 * core}
 
     def slot(k, src):
@@ -136,46 +146,49 @@
     def index(zz, yy, cc):
         return (zz * 2 + yy) * 2 + cc
 
-    def from_below(d):
-        return index(z - d, y, core)
-
-    def from_above(d):
-        return index(z + d, y, core)
-
     def own(k, act_on):
         act_on(k, sp, SIDE)
         pl.when(has_up)(lambda: act_on(k, sp, UP))
         pl.when(has_down)(lambda: act_on(k, sp, DOWN))
         act_on(k, sp, CORE)
 
-    def line(k, act_on, wait):
-        for d in range(1, levels):
-            @pl.when(z - d >= 0)
-            def _():
+    def line(k, act_on, wait, steps=None):
+        def one(src, way, more, to_side):
+            if wait:
+                copy(k, src, way).wait_recv()
+            if to_side is not None:
+                pl.when(to_side)(lambda: act_on(k, src, SIDE))
+            else:
+                act_on(k, src, SIDE)
+            pl.when(more)(lambda: act_on(k, src, way))
+            act_on(k, src, CORE)
+
+        paired = k in PAIRED
+        for d in steps or range(1, levels):
+            near = paired and d == 1
+            pl.when(z - d >= 0)(lambda: one(index(z - d, y, core), UP, has_up, even if near else None))
+            pl.when(z + d < levels)(lambda: one(index(z + d, y, core), DOWN, has_down, odd if near else None))
+            if d == 1:
+                first = index(z, 1 - y, core)
                 if wait:
-                    copy(k, from_below(d), UP).wait_recv()
-                act_on(k, from_below(d), SIDE)
-                pl.when(has_up)(lambda: act_on(k, from_below(d), UP))
-                act_on(k, from_below(d), CORE)
-
-            @pl.when(z + d < levels)
-            def _():
-                if wait:
-                    copy(k, from_above(d), DOWN).wait_recv()
-                act_on(k, from_above(d), SIDE)
-                pl.when(has_down)(lambda: act_on(k, from_above(d), DOWN))
-                act_on(k, from_above(d), CORE)
-
-    def across(k, act_on, wait):
-        def one(src):
+                    copy(k, first, SIDE).wait_recv()
+                if paired:
+                    pl.when(even)(lambda: act_on(k, first, UP))
+                    pl.when(odd)(lambda: act_on(k, first, DOWN))
+                act_on(k, first, CORE)
+
+    def across(k, act_on, wait, then=None):
+        def one(zz):
+            src = index(zz, 1 - y, core)
             if wait:
                 copy(k, src, SIDE).wait_recv()
             act_on(k, src, CORE)
-
-        one(index(z, 1 - y, core))
+            if then is not None:
+                then(zz, 1 - y)
+
         for d in range(1, levels):
-            pl.when(z - d >= 0)(lambda: one(index(z - d, 1 - y, core)))
-            pl.when(z + d < levels)(lambda: one(index(z + d, 1 - y, core)))
+            pl.when(z - d >= 0)(lambda: one(z - d))
+            pl.when(z + d < levels)(lambda: one(z + d))
 
     def other_core(k):
         for zz in range(levels):
@@ -217,15 +230,20 @@
     clo = lax.broadcasted_iota(jnp.int32, (LAYERS * width, width), 1)
     chi = lax.broadcasted_iota(jnp.int32, (LAYERS * width, width), 0)
 
-    for layer in range(LAYERS):
-        pick = (hi == LAYERS * lo + layer).astype(jnp.float32).astype(jnp.bfloat16)
-        for kind, ref in enumerate((v_ref, g_ref)):
+    def pick_rows(kind, ref):
+        for layer in range(LAYERS):
+            pick = (hi == LAYERS * lo + layer).astype(jnp.float32).astype(jnp.bfloat16)
             vg[layer * 2 + kind, sp] = jnp.dot(
                 pick, ref[...], preferred_element_type=jnp.float32).astype(jnp.bfloat16)
-        pick = (chi == LAYERS * clo + layer).astype(jnp.float32).astype(jnp.bfloat16)
-        ob[layer, sp] = jnp.dot(
-            o_ref[...], pick, preferred_element_type=jnp.float32).astype(jnp.bfloat16)
-    xf[tp] = x_ref[...]
+
+    def pick_columns():
+        for layer in range(LAYERS):
+            pick = (chi == LAYERS * clo + layer).astype(jnp.float32).astype(jnp.bfloat16)
+            ob[layer, sp] = jnp.dot(
+                o_ref[...], pick, preferred_element_type=jnp.float32).astype(jnp.bfloat16)
+
+    loads[0].wait()
+    pick_rows(0, v_ref)
 
     @pl.when(sp == 0)
     def _():
@@ -236,9 +254,17 @@
     pl.semaphore_wait(barrier, 3 + sum(end.astype(jnp.int32) for end in ends))
 
     own(0, start)
+    loads[2].wait()
     x_copy = to_peer(x_ref, xf.at[tp], (xsem.at[0], xsem.at[1]))
     x_copy.start()
+    loads[1].wait()
+    pick_rows(1, g_ref)
     own(1, start)
+    xf[tp] = x_ref[...]
+    loads[3].wait()
+    pick_columns()
+    for load in loads[4:]:
+        load.wait()
 
     def normalise(source, layer):
         total = jnp.zeros((rows, 1), jnp.float32)
@@ -281,7 +307,7 @@
             running = jnp.zeros((HALO, ch), jnp.float32)
             for k in range(KW):
                 at = r0 + k + HALO - (KW - 1)
-                running = running + taps_ref[layer, k : k + 1, tap_cols] * ext[layer, at : at + HALO]
+                running = running + taps_ref[k, layer : layer + 1, tap_cols] * ext[layer, at : at + HALO]
             cv[r0 : r0 + HALO] = running
 
         for r0 in range(HALO, rows, HALO):
@@ -315,6 +341,12 @@
     def add_parts(layer, p):
         return part[layer, p].astype(jnp.float32) + rpart[layer, p].astype(jnp.float32)
 
+    def project_last(zz, yy):
+        p = zz * 2 + yy
+        copy(ITEMS - 1, index(zz, yy, 1 - core), CORE).wait_recv()
+        project(LAYERS - 1, p)
+        pl.when(p // half_pairs == peer)(lambda: part_copy(LAYERS - 1, p).start())
+
     own(2, start)
     line(0, start, True)
     x_copy.wait_recv()
@@ -323,42 +355,46 @@
     line(1, start, True)
     across(0, start, True)
     own(4, start)
-    line(2, start, True)
+    near, far = range(1, levels - 1), range(levels - 1, levels)
+    line(2, start, True, near)
     across(1, start, True)
     own(5, start)
     other_core(0)
     other_core(1)
     glu(0)
-    line(3, start, True)
+    line(2, start, True, far)
+    line(3, start, True, near)
     conv(0)
+    line(3, start, True, far)
     across(2, start, True)
     activate(0)
     other_core(2)
     for p in range(pairs):
         project(0, p)
         part_copy(0, p).start()
-    line(4, start, True)
+        if p == half_pairs:
+            line(4, start, True, near)
+    line(4, start, True, far)
     across(3, start, True)
+    line(5, start, True)
     for p in range(pairs):
         part_copy(0, p).wait_recv()
         half, at = p // half_pairs, (p % half_pairs) * 2 * width
         here = xf[half, :, at : at + 2 * width].astype(jnp.float32)
         xn[half, :, at : at + 2 * width] = (here + add_parts(0, p)).astype(jnp.bfloat16)
     normalise(xn, 1)
-    line(5, start, True)
     across(4, start, True)
     other_core(3)
     other_core(4)
     glu(1)
     conv(1)
-    across(5, start, True)
     activate(1)
-    other_core(5)
-    for q in range(half_pairs):
-        project(1, peer * half_pairs + q)
-        part_copy(1, peer * half_pairs + q).start()
-    for q in range(half_pairs):
-        project(1, tp * half_pairs + q)
+    project_last(z, y)
+    for d in range(1, levels):
+        pl.when(z - d >= 0)(lambda: project_last(z - d, y))
+        pl.when(z + d < levels)(lambda: project_last(z + d, y))
+    project_last(z, 1 - y)
+    across(5, start, True, project_last)
     squares = jnp.zeros((rows, 1), jnp.float32)
     for q in range(half_pairs):
         p = tp * half_pairs + q
@@ -396,12 +432,15 @@
     width = out_weight.shape[1] // LAYERS
     bf16, f32 = jnp.bfloat16, jnp.float32
     dma = pltpu.SemaphoreType.DMA
+    arrays = (stream, norm_gain, value_weight, gate_weight, conv_taps.transpose(1, 0, 2),
+              ln_gain, ln_bias, out_weight, final_gain.reshape(1, -1))
     return pl.pallas_call(
         functools.partial(fused_kernel, n),
         out_shape=jax.ShapeDtypeStruct((rows, cols), bf16),
-        in_specs=[pl.BlockSpec(memory_space=pltpu.VMEM)] * 9,
+        in_specs=[pl.BlockSpec(memory_space=pl.ANY)] * 9,
         out_specs=pl.BlockSpec(memory_space=pltpu.VMEM),
-        scratch_shapes=[
+        scratch_shapes=[pltpu.VMEM(array.shape, array.dtype) for array in arrays] + [
+            dma((len(arrays),)),
             pltpu.VMEM((2 * LAYERS, n, depth, ch), bf16),
             pltpu.VMEM((LAYERS, n, ch, width), bf16),
             pltpu.VMEM((2, rows, cols), bf16),
@@ -422,8 +461,7 @@
             dma((LAYERS, 2, n // 2)),
         ],
         compiler_params=pltpu.CompilerParams(collective_id=0, has_side_effects=True),
-    )(stream, norm_gain, value_weight, gate_weight, conv_taps, ln_gain, ln_bias, out_weight,
-      final_gain.reshape(1, -1))
+    )(*arrays)
 
 
 def solution(mesh):
@@ -432,7 +470,7 @@
 
     def step(*args):
         stream, out_weight = args[0], args[7]
-        fits = n_tp == 2 and n % 4 == 0 and stream.shape[0] == 128 and out_weight.shape[1] == 128 * LAYERS
+        fits = n_tp == 2 and n % 8 == 0 and stream.shape[0] == 128 and out_weight.shape[1] == 128 * LAYERS
         return fused(n, *args) if fits else local(*args)
 
     return jax.shard_map(step, mesh=mesh, in_specs=placed, out_specs=P("sp", "tp"), check_vma=False)

time: 101 us -> 93 us (0.921)
  Pallas kernels: 97.4 us -> 90.9 us
  local copies, waits for them, and re-layouts: 3.41 us -> 1.67 us
    pallas_call x1, Pallas kernels: 97.4 us -> 90.9 us  [fused(): pl.pallas_call(functools.partial(fused_kernel, n), out_shape=jax.ShapeDty...]
    unnamed x2 -> x1, local copies, waits for them, and re-layouts: 3.41 us -> 1.67 us
where the time goes in v2:
time: 93 us; the launch traced here: 92.6 us
  Pallas kernels  90.9 us (98%)
  local copies, waits for them, and re-layouts  1.67 us (2%)
    pallas_call x1, Pallas kernels, fused(): pl.pallas_call(functools.partial(fused_kernel, n), out_shape=jax.ShapeDty...  90.9 us

profile of v2, /device:TPU:8, one launch (start us, length us, event | category | flops | bytes accessed | tf_op | source)
XLA Modules:
  0.0 92.6 jit_solution(14717096316596971419)
XLA Ops:
  0.0 90.9 %shard_map.91 = bf16[128,1024]{1,0:T(8,128)(2,1)} custom-call(bf16[128,1024]{1,0:T(8,128)(2,1)} %x_in.1, f32[2,2048]{1,0:T(2,128)} %ng_in.1, bf16[256,512]{1,0:T(8,128)(2,1)} %v_in.1, bf16[256,512]{1,0:T(8,128)(2,1)} %g_in.1, f32[31,2,1024]{2,1,0:T(2,128)} %bitcast.2, f32[2,1024]{1,0:T(2,128)} %lng_in.1, f32[2,1024]{1,0:T(2,128)} %lnb_in.1, ...), custom_call_target="tpu_custom_call" | custom-call | tf_op jit(solution)/shard_map/pallas_call | solution.py:437
  90.9 1.7 %copy.11 = bf16[128,1024]{1,0:T(8,128)(2,1)} copy(bf16[128,1024]{1,0:T(8,128)(2,1)} %shard_map.91) | data formatting | bytes 524288
